TPU v7x, 128 devices: a whole 4x4x4 slice. The times are simulated.
128 devices in a mesh: sp: 16 (over z, y), dp: 8 (over x, core).
Axes of the slice: x: 4, y: 4, z: 4, core: 2. Of those that a mesh axis runs over, the one named last changes fastest.
Arguments:
- query_first: bfloat16 [8, 2048, 1024], P('dp', 'sp'), may hold values from -200 to 200
- key_first: bfloat16 [8, 2048, 1024], P('dp', 'sp'), may hold values from -8 to 8
- query_second: bfloat16 [8, 2048, 1024], P('dp', 'sp'), may hold values from -200 to 200
- key_second: bfloat16 [8, 2048, 1024], P('dp', 'sp'), may hold values from -8 to 8
- value_rows: bfloat16 [8, 2048, 2048], P('dp', 'sp'), may hold values from -6 to 6
- mix_lambda: float32 [16], replicated, may hold values from 0.3 to 0.8
- head_gain: float32 [128], replicated, may hold values from 0.1 to 1.9
- residual: bfloat16 [8, 2048, 2048], P('dp', 'sp'), may hold values from -6 to 6
- out_weight: bfloat16 [2048, 2048], replicated, may hold values from -0.125 to 0.125
- norm_gain: float32 [2048], replicated, may hold values from 0.1 to 1.9
- routes: int32 [8, 2048, 4], P('dp', 'sp'), may hold values from 0 to 127, all different within a row; in each aligned block of 128 rows (0 to 127, 128 to 255, ..., all dimensions but the last counted through in order) at most 6 rows name the same one
- route_weights: float32 [8, 2048, 4], P('dp', 'sp'), may hold values from 0.1 to 1
- gate_weight: bfloat16 [128, 2048, 1024], P(('sp', 'dp')), may hold values from -0.375 to 0.375
- up_weight: bfloat16 [128, 2048, 1024], P(('sp', 'dp')), may hold values from -0.375 to 0.375
- down_weight: bfloat16 [128, 1024, 2048], P(('sp', 'dp')), may hold values from -0.046875 to 0.046875
Outputs:
- layer_out: bfloat16 [8, 2048, 2048], P('dp', 'sp')
Inputs may be any that keep to these rules, and one draw needn't show every extreme that they name: `routes`: within the rows of one device (aligned blocks of 128 positions of a sequence) no expert is named more than 6 times, a bound that some block reaches.
All inputs are finite; a program needn't handle non-finite values.
Results may differ from a plain program's by a relative error of at most 0.0075.
Values may be sent and summed in bfloat16 or wider, within the bound.
No kernel may reach another device: no remote copies, remote signals or barrier semaphores. Data moves between devices by JAX's collectives and lax.ppermute only.
A program may use at most 128 MiB of HBM per device.

v0:
```python
import functools

import jax
import jax.numpy as jnp
from jax import lax
from jax.experimental import pallas as pl
from jax.experimental.pallas import tpu as pltpu
from jax.sharding import PartitionSpec as P

BF = jnp.bfloat16
F32 = jnp.float32
LANES = 128
SLOTS = 6
ROWS = 8
MIB = 1024 * 1024


def dot(a, b, dims=((1,), (0,))):
    return lax.dot_general(a, b, (dims, ((), ())), preferred_element_type=F32)


def vmem_specs(count):
    return [pl.BlockSpec(memory_space=pltpu.VMEM)] * count


def pack_kernel(q1_ref, k1_ref, q2_ref, k2_ref, v_ref, out_ref):
    tok = q1_ref.shape[0]
    heads = v_ref.shape[1] // LANES
    half = LANES // 2
    for h in range(heads):
        rows = slice(h * tok, (h + 1) * tok)
        cols = slice(h * half, (h + 1) * half)
        out_ref[rows, 0:LANES] = jnp.concatenate([q1_ref[:, cols], q2_ref[:, cols]], axis=1)
        out_ref[rows, LANES : 2 * LANES] = jnp.concatenate(
            [k1_ref[:, cols], k2_ref[:, cols]], axis=1
        )
        out_ref[rows, 2 * LANES : 3 * LANES] = v_ref[:, h * LANES : (h + 1) * LANES]


def pack_heads(q1, k1, q2, k2, v):
    tok = q1.shape[0]
    heads = v.shape[1] // LANES
    return pl.pallas_call(
        pack_kernel,
        out_shape=jax.ShapeDtypeStruct((heads * tok, 3 * LANES), BF),
        in_specs=vmem_specs(5),
        out_specs=pl.BlockSpec(memory_space=pltpu.VMEM),
        compiler_params=pltpu.CompilerParams(vmem_limit_bytes=8 * MIB),
        name="pack_heads",
    )(q1, k1, q2, k2, v)


def attention_kernel(lam_ref, gain_ref, qkv_ref, out_ref, *, block):
    length = qkv_ref.shape[0]
    half = LANES // 2
    scale = (half**-0.5) * 1.4426950408889634
    lane = lax.broadcasted_iota(jnp.int32, (block, LANES), 1)
    causal = lax.broadcasted_iota(jnp.int32, (2 * block, block), 1) <= (
        lax.broadcasted_iota(jnp.int32, (2 * block, block), 0) & (block - 1)
    )
    lam = lam_ref[0, 0]
    gain = gain_ref[...]
    for step in range(length // block):
        rows = slice(step * block, (step + 1) * block)
        queries = qkv_ref[rows, 0:LANES]
        zero = jnp.zeros_like(queries)
        both = jnp.concatenate(
            [jnp.where(lane < half, queries, zero), jnp.where(lane < half, zero, queries)], axis=0
        )
        scores = []
        for c in range(step + 1):
            keys = qkv_ref[c * block : (c + 1) * block, LANES : 2 * LANES]
            s = dot(both, keys, ((1,), (1,)))
            if c == step:
                s = jnp.where(causal, s, -1e30)
            scores.append(s)
        top = functools.reduce(jnp.maximum, scores)
        top = jnp.max(top, axis=1, keepdims=True)
        total = None
        raw = None
        for c in range(step + 1):
            p = jnp.exp2((scores[c] - top) * scale)
            total = p if total is None else total + p
            values = qkv_ref[c * block : (c + 1) * block, 2 * LANES : 3 * LANES]
            part = dot(p.astype(BF), values)
            raw = part if raw is None else raw + part
        total = jnp.sum(total, axis=1, keepdims=True)
        normal = raw / total
        head = normal[:block] - lam * normal[block:]
        factor = lax.rsqrt(jnp.mean(head * head, axis=1, keepdims=True) + 1e-06)
        out_ref[rows, :] = (head * factor * gain).astype(BF)


def attention(lam, gain, qkv):
    length = qkv.shape[0]
    return pl.pallas_call(
        functools.partial(attention_kernel, block=256),
        out_shape=jax.ShapeDtypeStruct((length, LANES), BF),
        in_specs=[pl.BlockSpec(memory_space=pltpu.SMEM)] + vmem_specs(2),
        out_specs=pl.BlockSpec(memory_space=pltpu.VMEM),
        compiler_params=pltpu.CompilerParams(vmem_limit_bytes=24 * MIB),
        name="attention",
    )(lam, gain, qkv)


def route_kernel(routes_ref, weights_ref, send_ref, mix_ref):
    topk, tok = routes_ref.shape
    experts = send_ref.shape[0] // ROWS
    expert = lax.broadcasted_iota(jnp.int32, (experts, tok), 0)
    named = jnp.zeros((experts, tok), F32)
    weight = jnp.zeros((experts, tok), F32)
    for k in range(topk):
        hit = expert == routes_ref[k : k + 1, :]
        named = jnp.where(hit, 1.0, named)
        weight = jnp.where(hit, weights_ref[k : k + 1, :], weight)
    before = lax.broadcasted_iota(jnp.int32, (tok, tok), 0) < lax.broadcasted_iota(
        jnp.int32, (tok, tok), 1
    )
    rank = dot(named.astype(BF), jnp.where(before, 1.0, 0.0).astype(BF))
    slot = jnp.where(named > 0.0, rank, -9.0)
    high = weight.astype(BF)
    low = (weight - high.astype(F32)).astype(BF)

    def spread(x):
        x = jnp.broadcast_to(x[:, None, :], (experts, ROWS, tok))
        return x.reshape(experts * ROWS, tok)

    slot = spread(slot)
    high = spread(high.astype(F32))
    low = spread(low.astype(F32))
    row = lax.broadcasted_iota(jnp.int32, (experts * ROWS, tok), 0) & (ROWS - 1)
    for part in range(4):
        if part == 0:
            wanted = jnp.where(row < SLOTS, row, -1)
        else:
            wanted = jnp.where(row < SLOTS, -1, row - SLOTS + 2 * (part - 1))
        hit = slot == wanted.astype(F32)
        send_ref[:, part * tok : (part + 1) * tok] = jnp.where(hit, 1.0, 0.0).astype(BF)
        base = part * 2 * tok
        mix_ref[base : base + tok, :] = jnp.where(hit, high, 0.0).T.astype(BF)
        mix_ref[base + tok : base + 2 * tok, :] = jnp.where(hit, low, 0.0).T.astype(BF)


def route_tables(routes, weights, experts):
    topk, tok = routes.shape
    return pl.pallas_call(
        route_kernel,
        out_shape=(
            jax.ShapeDtypeStruct((experts * ROWS, 4 * tok), BF),
            jax.ShapeDtypeStruct((8 * tok, experts * ROWS), BF),
        ),
        in_specs=vmem_specs(2),
        out_specs=tuple(vmem_specs(2)),
        compiler_params=pltpu.CompilerParams(vmem_limit_bytes=16 * MIB),
        name="route_tables",
    )(routes, weights)


def middle_kernel(heads_ref, weight_ref, residual_ref, gain_ref, send_ref, mixed_ref, out_ref):
    tok, width = residual_ref.shape
    heads = heads_ref.shape[0] // tok
    joined = jnp.concatenate(
        [heads_ref[h * tok : (h + 1) * tok, :] for h in range(heads)], axis=1
    )
    tile = 256
    square = jnp.zeros((tok, tile), F32)
    for n in range(width // tile):
        cols = slice(n * tile, (n + 1) * tile)
        mixed = residual_ref[:, cols].astype(F32) + dot(joined, weight_ref[:, cols])
        mixed_ref[:, cols] = mixed
        square = square + mixed * mixed
    factor = lax.rsqrt(jnp.sum(square, axis=1, keepdims=True) / width + 1e-06)
    normed = (mixed_ref[...] * factor * gain_ref[...]).astype(BF)
    part = width // 4
    for q in range(3):
        rows = jnp.concatenate(
            [normed[:, q * part : (q + 1) * part], normed[:, 3 * part :]], axis=0
        )
        chosen = jnp.concatenate(
            [send_ref[:, 0:tok], send_ref[:, (q + 1) * tok : (q + 2) * tok]], axis=1
        )
        out_ref[:, q * part : (q + 1) * part] = dot(chosen, rows).astype(BF)


def middle(heads, weight, residual, gain, send):
    tok, width = residual.shape
    return pl.pallas_call(
        middle_kernel,
        out_shape=(
            jax.ShapeDtypeStruct((tok, width), F32),
            jax.ShapeDtypeStruct((send.shape[0], 3 * width // 4), BF),
        ),
        in_specs=vmem_specs(5),
        out_specs=tuple(vmem_specs(2)),
        compiler_params=pltpu.CompilerParams(vmem_limit_bytes=24 * MIB),
        name="middle",
    )(heads, weight, residual, gain, send)


def moved(x, shift):
    rows, cols = x.shape
    return pltpu.roll(x.reshape(rows // ROWS, ROWS, cols), shift, 1).reshape(rows, cols)


def experts_kernel(x_ref, gate_ref, up_ref, down_ref, out_ref, tail_ref, hidden_ref, last_ref):
    step = pl.program_id(0)
    rows = x_ref.shape[0]
    part = x_ref.shape[1] // 3
    tile = gate_ref.shape[1]
    gates = hidden_ref.shape[0]
    row = lax.broadcasted_iota(jnp.int32, (rows, part), 0) & (ROWS - 1)

    @pl.when(step == 0)
    def _():
        first = moved(x_ref[:, 0:part].astype(F32), 2)
        second = moved(x_ref[:, part : 2 * part].astype(F32), 4)
        third = moved(x_ref[:, 2 * part : 3 * part].astype(F32), 6)
        tail = jnp.where(row < 2, first, jnp.where(row < 4, second, third))
        tail_ref[...] = jnp.where(row < SLOTS, tail, 0.0).astype(BF)

    @pl.when(step < gates)
    def _():
        def times(w_ref):
            return dot(x_ref[...], w_ref[0 : 3 * part, :]) + dot(tail_ref[...], w_ref[3 * part :, :])

        gate = jnp.minimum(times(gate_ref), 7.0)
        up = jnp.clip(times(up_ref), -7.0, 7.0) + 1.0
        hidden_ref[step] = (up * gate * jax.nn.sigmoid(1.702 * gate)).astype(BF)

    def result():
        total = None
        for g in range(gates):
            term = dot(hidden_ref[g], down_ref[g * tile : (g + 1) * tile, :])
            total = term if total is None else total + term
        return total

    @pl.when(step == gates)
    def _():
        last_ref[...] = result()

    for q in range(3):

        @pl.when(step == gates + 1 + q)
        def _():
            out_ref[...] = jnp.where(
                row < SLOTS, result(), moved(last_ref[...], SLOTS - 2 * q)
            ).astype(BF)


def experts(x, gate_weight, up_weight, down_weight):
    rows = x.shape[0]
    width, hidden = gate_weight.shape
    part = width // 4
    tile = 256
    gates = hidden // tile

    def gate_map(i):
        return (0, jnp.minimum(i, gates - 1))

    def down_map(i):
        return (0, jnp.where(i <= gates, 3, i - gates - 1))

    def out_map(i):
        return (0, jnp.maximum(i - gates - 1, 0))

    return pl.pallas_call(
        experts_kernel,
        grid=(gates + 4,),
        out_shape=jax.ShapeDtypeStruct((rows, 3 * part), BF),
        in_specs=[
            pl.BlockSpec((rows, 3 * part), lambda i: (0, 0)),
            pl.BlockSpec((width, tile), gate_map),
            pl.BlockSpec((width, tile), gate_map),
            pl.BlockSpec((hidden, part), down_map),
        ],
        out_specs=pl.BlockSpec((rows, part), out_map),
        scratch_shapes=[
            pltpu.VMEM((rows, part), BF),
            pltpu.VMEM((gates, rows, tile), BF),
            pltpu.VMEM((rows, part), F32),
        ],
        compiler_params=pltpu.CompilerParams(vmem_limit_bytes=40 * MIB),
        name="experts",
    )(x, gate_weight, up_weight, down_weight)


def combine_kernel(mixed_ref, rows_ref, mix_ref, out_ref):
    tok, width = mixed_ref.shape
    part = width // 4
    last = mixed_ref[:, 3 * part :]
    for q in range(3):
        cols = slice(q * part, (q + 1) * part)
        weights = jnp.concatenate(
            [mix_ref[0 : 2 * tok, :], mix_ref[(q + 1) * 2 * tok : (q + 2) * 2 * tok, :]], axis=0
        )
        sums = dot(weights, rows_ref[:, cols])
        out_ref[:, cols] = (mixed_ref[:, cols] + sums[0:tok] + sums[tok : 2 * tok]).astype(BF)
        last = last + sums[2 * tok : 3 * tok] + sums[3 * tok :]
    out_ref[:, 3 * part :] = last.astype(BF)


def combine(mixed, rows, mix):
    return pl.pallas_call(
        combine_kernel,
        out_shape=jax.ShapeDtypeStruct(mixed.shape, BF),
        in_specs=vmem_specs(3),
        out_specs=pl.BlockSpec(memory_space=pltpu.VMEM),
        compiler_params=pltpu.CompilerParams(vmem_limit_bytes=24 * MIB),
        name="combine",
    )(mixed, rows, mix)


def exchange(x, axis, devices):
    pieces = x.reshape(devices, x.shape[0] // devices, x.shape[1])
    out = lax.all_to_all(pieces, axis, split_axis=0, concat_axis=0, tiled=True)
    return out.reshape(x.shape)


def on_device(
    query_first,
    key_first,
    query_second,
    key_second,
    value_rows,
    mix_lambda,
    head_gain,
    residual,
    out_weight,
    norm_gain,
    routes,
    route_weights,
    gate_weight,
    up_weight,
    down_weight,
):
    along = lax.axis_size("sp")
    everyone = along * lax.axis_size("dp")
    packed = pack_heads(
        query_first[0], key_first[0], query_second[0], key_second[0], value_rows[0]
    )
    qkv = exchange(packed, "sp", along)
    lam = lax.dynamic_slice_in_dim(mix_lambda, lax.axis_index("sp"), 1).reshape(1, 1)
    send, mix = route_tables(routes[0].T, route_weights[0].T, everyone)
    heads = exchange(attention(lam, head_gain.reshape(1, -1), qkv), "sp", along)
    mixed, outgoing = middle(heads, out_weight, residual[0], norm_gain.reshape(1, -1), send)
    received = exchange(outgoing, ("sp", "dp"), everyone)
    finished = experts(received, gate_weight[0], up_weight[0], down_weight[0])
    returned = exchange(finished, ("sp", "dp"), everyone)
    return combine(mixed, returned, mix)[None]


def solution(mesh):
    split = P("dp", "sp", None)
    held = P(("sp", "dp"), None, None)
    return jax.shard_map(
        on_device,
        mesh=mesh,
        in_specs=(split,) * 5 + (P(), P(), split, P(), P(), split, split) + (held,) * 3,
        out_specs=split,
        check_vma=False,
    )
```

profile of v0, /device:TPU:1, one launch (start us, length us, event | category | flops | bytes accessed | tf_op | source)
XLA Modules:
  0.0 183.9 jit_solution(15646116903701564292)
XLA Ops:
  0.0 1.0 copy-done.5
  1.0 0.9 copy-done.6
  2.0 0.9 copy-done.7
  2.9 0.9 copy-done.8
  3.9 0.9 copy-done.9
  4.8 1.6 pack_heads.1
  6.4 8.7 %all-to-all-start = ((bf16[16,128,384]{2,1,0:T(8,128)(2,1)}), bf16[16,128,384]{2,1,0:T(8,128)(2,1)S(1)}, u32[]{:S(2)}, u32[]{:S(2)}) async-start(bf16[16,128,384]{2,1,0:T(8,128)(2,1)} %bitcast.7), calls=%async_computation | async-start | bytes 3145728 | tf_op jit(solution)/shard_map/all_to_all | solution.py:315
  15.2 0.0 copy-done.14
  15.2 0.6 dynamic_slice.3
  15.7 22.5 %all-to-all-done = bf16[16,128,384]{2,1,0:T(8,128)(2,1)S(1)} async-done(((bf16[16,128,384]{2,1,0:T(8,128)(2,1)}), bf16[16,128,384]{2,1,0:T(8,128)(2,1)S(1)}, u32[]{:S(2)}, u32[]{:S(2)}) %all-to-all-start) | async-done | bytes 1572896 | tf_op jit(solution)/shard_map/all_to_all | solution.py:315
  38.3 0.0 copy-done.13
  38.3 8.8 %attention.1 = bf16[2048,128]{1,0:T(8,128)(2,1)} custom-call(f32[1,1]{1,0:T(1,128)} %bitcast.lam_ref, f32[1,128]{1,0:T(1,128)S(1)} %bitcast.43, bf16[2048,384]{1,0:T(8,128)(2,1)S(1)} %bitcast.30), custom_call_target="tpu_custom_call" | custom-call | tf_op jit(solution)/shard_map/attention/pallas_call | solution.py:96
  47.1 4.5 %all-to-all-start.1 = ((bf16[16,128,128]{2,1,0:T(8,128)(2,1)}), bf16[16,128,128]{2,1,0:T(8,128)(2,1)S(1)}, u32[]{:S(2)}, u32[]{:S(2)}) async-start(bf16[16,128,128]{2,1,0:T(8,128)(2,1)} %bitcast.9), calls=%async_computation.1 | async-start | bytes 1048576 | tf_op jit(solution)/shard_map/all_to_all | solution.py:315
  51.6 1.4 route_tables.1
  53.0 1.0 copy-done.2
  54.0 7.8 %all-to-all-done.1 = bf16[16,128,128]{2,1,0:T(8,128)(2,1)S(1)} async-done(((bf16[16,128,128]{2,1,0:T(8,128)(2,1)}), bf16[16,128,128]{2,1,0:T(8,128)(2,1)S(1)}, u32[]{:S(2)}, u32[]{:S(2)}) %all-to-all-start.1) | async-done | bytes 524320 | tf_op jit(solution)/shard_map/all_to_all | solution.py:315
  61.8 3.4 %copy-done = bf16[2048,2048]{1,0:T(8,128)(2,1)S(1)} copy-done((bf16[2048,2048]{1,0:T(8,128)(2,1)S(1)}, bf16[2048,2048]{1,0:T(8,128)(2,1)}, u32[]{:S(2)}) %copy-start) | copy-done | bytes 8388632
  65.1 1.2 copy-done.3
  66.4 2.4 %middle.1 = (f32[128,2048]{1,0:T(8,128)S(1)}, bf16[1024,1536]{1,0:T(8,128)(2,1)S(1)}) custom-call(bf16[2048,128]{1,0:T(8,128)(2,1)S(1)} %bitcast.33, bf16[2048,2048]{1,0:T(8,128)(2,1)S(1)} %copy-done, bf16[128,2048]{1,0:T(8,128)(2,1)S(1)} %bitcast.34, f32[1,2048]{1,0:T(1,128)S(1)} %bitcast.40, bf16[1024,512]{1,0:T(8,128)(2,1)S(1)} %copy-done.3), custom_call_target="tpu_custom_call" | custom-call | tf_op jit(solution)/shard_map/middle/pallas_call | solution.py:187
  68.7 0.0 copy-start.1
  68.8 48.7 %all_to_all.20 = bf16[128,8,1536]{2,1,0:T(8,128)(2,1)S(1)} all-to-all(bf16[128,8,1536]{2,1,0:T(8,128)(2,1)S(1)} %bitcast.32), channel_id=1, replica_groups=mesh['sp'=16,'dp'=8] {'sp','dp'}, dimensions={0} | all-to-all | bytes 6291456 | tf_op jit(solution)/shard_map/all_to_all | solution.py:315
  117.4 18.3 %experts.1 = bf16[1024,1536]{1,0:T(8,128)(2,1)S(1)} custom-call(bf16[1024,1536]{1,0:T(8,128)(2,1)S(1)} %bitcast.27, bf16[2048,1024]{1,0:T(8,128)(2,1)S(1)} %bitcast.31, bf16[2048,1024]{1,0:T(8,128)(2,1)} %bitcast.44, bf16[1024,2048]{1,0:T(8,128)(2,1)} %bitcast.45), custom_call_target="tpu_custom_call" | custom-call | tf_op jit(solution)/shard_map/experts/pallas_call | solution.py:266
  135.7 45.6 %all_to_all.21 = bf16[128,8,1536]{2,1,0:T(8,128)(2,1)S(1)} all-to-all(bf16[128,8,1536]{2,1,0:T(8,128)(2,1)S(1)} %bitcast.28), channel_id=1, replica_groups=mesh['sp'=16,'dp'=8] {'sp','dp'}, dimensions={0} | all-to-all | bytes 6291456 | tf_op jit(solution)/shard_map/all_to_all | solution.py:315
  181.3 2.6 %combine.1 = bf16[128,2048]{1,0:T(8,128)(2,1)} custom-call(f32[128,2048]{1,0:T(8,128)S(1)} %get-tuple-element.10.mixed_ref, bf16[1024,1536]{1,0:T(8,128)(2,1)S(1)} %bitcast.29, bf16[1024,1024]{1,0:T(8,128)(2,1)S(1)} %get-tuple-element.12.mix_ref), custom_call_target="tpu_custom_call" | custom-call | tf_op jit(solution)/shard_map/combine/pallas_call | solution.py:303
  (19 shorter events, 0.0 us)
Async XLA Ops:
  0.0 1.0 copy-start.5
  1.0 0.9 copy-start.6
  2.0 0.9 copy-start.7
  2.9 0.9 copy-start.8
  3.9 0.9 copy-start.9
  4.8 10.3 %copy-start.14 = (f32[16]{0:T(128)S(1)}, f32[16]{0:T(128)}, u32[]{:S(2)}) copy-start(f32[16]{0:T(128)} %param.20) | copy-start | bytes 196
  4.8 33.4 %copy-start.13 = (f32[128]{0:T(128)S(1)}, f32[128]{0:T(128)}, u32[]{:S(2)}) copy-start(f32[128]{0:T(128)} %param.21) | copy-start | bytes 1540
  6.4 45.1 %copy-start.11 = (s32[1,128,4]{1,2,0:T(4,128)S(1)}, s32[1,128,4]{1,2,0:T(4,128)}, u32[]{:S(2)}) copy-start(s32[1,128,4]{1,2,0:T(4,128)} %param.25) | copy-start | bytes 6148
  6.4 45.1 %copy-start.12 = (f32[1,128,4]{1,2,0:T(4,128)S(1)}, f32[1,128,4]{1,2,0:T(4,128)}, u32[]{:S(2)}) copy-start(f32[1,128,4]{1,2,0:T(4,128)} %param.26) | copy-start | bytes 6148
  6.4 55.3 %copy-start.4 = (bf16[1,128,2048]{2,1,0:T(8,128)(2,1)S(1)}, bf16[1,128,2048]{2,1,0:T(8,128)(2,1)}, u32[]{:S(2)}) copy-start(bf16[1,128,2048]{2,1,0:T(8,128)(2,1)} %param.22) | copy-start | bytes 1572868
  6.4 55.3 %copy-start.10 = (f32[2048]{0:T(1024)S(1)}, f32[2048]{0:T(1024)}, u32[]{:S(2)}) copy-start(f32[2048]{0:T(1024)} %param.24) | copy-start | bytes 24580
  6.4 31.8 %all-to-all-start = ((bf16[16,128,384]{2,1,0:T(8,128)(2,1)}), bf16[16,128,384]{2,1,0:T(8,128)(2,1)S(1)}, u32[]{:S(2)}, u32[]{:S(2)}) async-start(bf16[16,128,384]{2,1,0:T(8,128)(2,1)} %bitcast.7), calls=%async_computation | async-start | bytes 3145728 | tf_op jit(solution)/shard_map/all_to_all | solution.py:315
  47.1 14.6 %all-to-all-start.1 = ((bf16[16,128,128]{2,1,0:T(8,128)(2,1)}), bf16[16,128,128]{2,1,0:T(8,128)(2,1)S(1)}, u32[]{:S(2)}, u32[]{:S(2)}) async-start(bf16[16,128,128]{2,1,0:T(8,128)(2,1)} %bitcast.9), calls=%async_computation.1 | async-start | bytes 1048576 | tf_op jit(solution)/shard_map/all_to_all | solution.py:315
  53.0 1.0 copy-start.2
  61.8 3.4 %copy-start = (bf16[2048,2048]{1,0:T(8,128)(2,1)S(1)}, bf16[2048,2048]{1,0:T(8,128)(2,1)}, u32[]{:S(2)}) copy-start(bf16[2048,2048]{1,0:T(8,128)(2,1)} %weight_ref.1) | copy-start | bytes 25165828
  65.1 1.2 copy-start.3
  68.7 48.7 %copy-start.1 = (bf16[1,2048,1024]{2,1,0:T(8,128)(2,1)S(1)}, bf16[1,2048,1024]{2,1,0:T(8,128)(2,1)}, u32[]{:S(2)}) copy-start(bf16[1,2048,1024]{2,1,0:T(8,128)(2,1)} %param.27) | copy-start | bytes 12582916
where the time goes:
time: 184 us
  blocking collectives  94.3 us (51%)
  Pallas kernels  35 us (19%)
  waiting for transfers between devices  30.3 us (16%)
  starting transfers between devices  13.2 us (7%)
  local copies, waits for them, and re-layouts  11 us (6%)
    all_to_all x2, blocking collectives, exchange(): out = lax.all_to_all(pieces, axis, split_axis=0, concat_axis=0, tiled=True)  94.3 us
    all_to_all x2, waiting for transfers between devices, exchange(): out = lax.all_to_all(pieces, axis, split_axis=0, concat_axis=0, tiled=True)  30.3 us
    pallas_call x1, Pallas kernels, experts(): pl.pallas_call(experts_kernel, grid=(gates + 4,), out_shape=jax.ShapeDtyp...  18.3 us
    all_to_all x2, starting transfers between devices, exchange(): out = lax.all_to_all(pieces, axis, split_axis=0, concat_axis=0, tiled=True)  13.2 us
    unnamed x30, local copies, waits for them, and re-layouts  10.5 us
    pallas_call x1, Pallas kernels, attention(): pl.pallas_call(functools.partial(attention_kernel, block=256), out_shape=...  8.84 us
  transfers between devices with their start and end apart: 2, of which 2 were waited for; matrix products, arithmetic and copies ran while one was open for 0% of the time, Pallas kernels for 1%

commit v1 on v0

v1 whole, which is shorter than its diff:
```python
import functools

import jax
import jax.numpy as jnp
from jax import lax
from jax.experimental import pallas as pl
from jax.experimental.pallas import tpu as pltpu
from jax.sharding import PartitionSpec as P

BF = jnp.bfloat16
F32 = jnp.float32
LANES = 128
SLOTS = 6
ROWS = 8
MIB = 1024 * 1024


def dot(a, b, dims=((1,), (0,))):
    return lax.dot_general(a, b, (dims, ((), ())), preferred_element_type=F32)


def in_hbm(*arrays):
    return [pltpu.with_memory_space_constraint(a, pltpu.HBM) for a in arrays]


def vmem_specs(count):
    return [pl.BlockSpec(memory_space=pltpu.VMEM)] * count


def pack_kernel(q1_hbm, k1_hbm, q2_hbm, k2_hbm, v_hbm, out_ref, q1_ref, k1_ref, q2_ref, k2_ref, v_ref, sems):
    tok = q1_ref.shape[0]
    heads = v_ref.shape[1] // LANES
    half = LANES // 2
    pairs = ((q1_hbm, q1_ref), (q2_hbm, q2_ref), (k1_hbm, k1_ref), (k2_hbm, k2_ref), (v_hbm, v_ref))
    copies = [pltpu.make_async_copy(a, b, sems.at[i]) for i, (a, b) in enumerate(pairs)]
    for copy in copies:
        copy.start()
    for begin, (first, second) in ((0, (q1_ref, q2_ref)), (1, (k1_ref, k2_ref))):
        copies[2 * begin].wait()
        copies[2 * begin + 1].wait()
        lanes = slice(begin * LANES, (begin + 1) * LANES)
        for h in range(heads):
            cols = slice(h * half, (h + 1) * half)
            out_ref[h * tok : (h + 1) * tok, lanes] = jnp.concatenate(
                [first[:, cols], second[:, cols]], axis=1
            )
    copies[4].wait()
    for h in range(heads):
        out_ref[h * tok : (h + 1) * tok, 2 * LANES : 3 * LANES] = v_ref[
            :, h * LANES : (h + 1) * LANES
        ]


def pack_heads(q1, k1, q2, k2, v):
    tok = q1.shape[0]
    heads = v.shape[1] // LANES
    return pl.pallas_call(
        pack_kernel,
        out_shape=jax.ShapeDtypeStruct((heads * tok, 3 * LANES), BF),
        in_specs=[pl.BlockSpec(memory_space=pltpu.HBM)] * 5,
        out_specs=pl.BlockSpec(memory_space=pltpu.VMEM),
        scratch_shapes=[pltpu.VMEM(x.shape, BF) for x in (q1, k1, q2, k2, v)]
        + [pltpu.SemaphoreType.DMA((5,))],
        compiler_params=pltpu.CompilerParams(vmem_limit_bytes=8 * MIB),
        name="pack_heads",
    )(*in_hbm(q1, k1, q2, k2, v))


def attention_kernel(
    lam_ref, gain_ref, qkv_ref, *refs, block
):
    held = (len(refs) - 2) // 2
    out_ref, sems = refs[held], refs[-1]
    loads = [
        pltpu.make_async_copy(refs[i], refs[held + 1 + i], sems.at[i]) for i in range(held)
    ]
    for load in loads:
        load.start()
    length = qkv_ref.shape[0]
    half = LANES // 2
    scale = (half**-0.5) * 1.4426950408889634
    lane = lax.broadcasted_iota(jnp.int32, (block, LANES), 1)
    causal = lax.broadcasted_iota(jnp.int32, (2 * block, block), 1) <= (
        lax.broadcasted_iota(jnp.int32, (2 * block, block), 0) & (block - 1)
    )
    lam = lam_ref[lax.axis_index("sp")]
    gain = gain_ref[...]
    for step in range(length // block):
        rows = slice(step * block, (step + 1) * block)
        queries = qkv_ref[rows, 0:LANES]
        zero = jnp.zeros_like(queries)
        both = jnp.concatenate(
            [jnp.where(lane < half, queries, zero), jnp.where(lane < half, zero, queries)], axis=0
        )
        scores = []
        for c in range(step + 1):
            keys = qkv_ref[c * block : (c + 1) * block, LANES : 2 * LANES]
            s = dot(both, keys, ((1,), (1,)))
            if c == step:
                s = jnp.where(causal, s, -1e30)
            scores.append(s)
        top = functools.reduce(jnp.maximum, scores)
        top = jnp.max(top, axis=1, keepdims=True)
        total = None
        raw = None
        for c in range(step + 1):
            p = jnp.exp2((scores[c] - top) * scale)
            total = p if total is None else total + p
            values = qkv_ref[c * block : (c + 1) * block, 2 * LANES : 3 * LANES]
            part = dot(p.astype(BF), values)
            raw = part if raw is None else raw + part
        total = jnp.sum(total, axis=1, keepdims=True)
        normal = raw / total
        head = normal[:block] - lam * normal[block:]
        factor = lax.rsqrt(jnp.mean(head * head, axis=1, keepdims=True) + 1e-06)
        out_ref[rows, :] = (head * factor * gain).astype(BF)
    for load in loads:
        load.wait()


def attention(lam, gain, qkv, *weights):
    length = qkv.shape[0]
    return pl.pallas_call(
        functools.partial(attention_kernel, block=256),
        out_shape=(jax.ShapeDtypeStruct((length, LANES), BF),)
        + tuple(pltpu.VMEM(w.shape, BF) for w in weights),
        in_specs=[pl.BlockSpec(memory_space=pltpu.SMEM)]
        + vmem_specs(2)
        + [pl.BlockSpec(memory_space=pltpu.HBM)] * len(weights),
        out_specs=tuple(vmem_specs(1 + len(weights))),
        scratch_shapes=[pltpu.SemaphoreType.DMA((len(weights),))],
        compiler_params=pltpu.CompilerParams(vmem_limit_bytes=24 * MIB),
        name="attention",
    )(lam, gain, qkv, *in_hbm(*weights))


def spread(x):
    experts, tok = x.shape
    x = jnp.broadcast_to(x[:, None, :], (experts, ROWS, tok))
    return x.reshape(experts * ROWS, tok)


def slot_hits(slot):
    experts, tok = slot.shape
    slot = spread(slot)
    row = lax.broadcasted_iota(jnp.int32, (experts * ROWS, tok), 0) & (ROWS - 1)
    for part in range(4):
        if part == 0:
            wanted = jnp.where(row < SLOTS, row, -1)
        else:
            wanted = jnp.where(row < SLOTS, -1, row - SLOTS + 2 * (part - 1))
        yield slot == wanted.astype(F32)


def slot_table(routes_ref, experts):
    topk, tok = routes_ref.shape
    expert = lax.broadcasted_iota(jnp.int32, (experts, tok), 0)
    named = jnp.zeros((experts, tok), F32)
    hits = [expert == routes_ref[k : k + 1, :] for k in range(topk)]
    for hit in hits:
        named = jnp.where(hit, 1.0, named)
    before = lax.broadcasted_iota(jnp.int32, (tok, tok), 0) < lax.broadcasted_iota(
        jnp.int32, (tok, tok), 1
    )
    rank = dot(named.astype(BF), jnp.where(before, 1.0, 0.0).astype(BF))
    return jnp.where(named > 0.0, rank, -9.0), hits


def mix_table(routes_ref, weights_ref, mix_ref):
    tok = routes_ref.shape[1]
    slot, hits = slot_table(routes_ref, mix_ref.shape[1] // ROWS)
    weight = jnp.zeros(slot.shape, F32)
    for k, hit in enumerate(hits):
        weight = jnp.where(hit, weights_ref[k : k + 1, :], weight)
    high = weight.astype(BF).astype(F32)
    low = spread(weight - high)
    high = spread(high)
    for part, hit in enumerate(slot_hits(slot)):
        base = part * 2 * tok
        mix_ref[base : base + tok, :] = jnp.where(hit, high, 0.0).T.astype(BF)
        mix_ref[base + tok : base + 2 * tok, :] = jnp.where(hit, low, 0.0).T.astype(BF)


def middle_kernel(
    heads_ref, weight_ref, residual_ref, gain_ref, routes_ref, mixed_ref, out_ref
):
    tok, width = residual_ref.shape
    heads = heads_ref.shape[0] // tok
    tile = 256
    slot, _ = slot_table(routes_ref, out_ref.shape[0] // ROWS)
    hits = [jnp.where(hit, 1.0, 0.0).astype(BF) for hit in slot_hits(slot)]
    joined = jnp.concatenate(
        [heads_ref[h * tok : (h + 1) * tok, :] for h in range(heads)], axis=1
    )
    square = jnp.zeros((tok, tile), F32)
    for n in range(width // tile):
        cols = slice(n * tile, (n + 1) * tile)
        mixed = residual_ref[:, cols].astype(F32) + dot(joined, weight_ref[:, cols])
        mixed_ref[:, cols] = mixed
        square = square + mixed * mixed
    factor = lax.rsqrt(jnp.sum(square, axis=1, keepdims=True) / width + 1e-06)
    normed = (mixed_ref[...] * factor * gain_ref[...]).astype(BF)
    part = width // 4
    for q in range(3):
        rows = jnp.concatenate(
            [normed[:, q * part : (q + 1) * part], normed[:, 3 * part :]], axis=0
        )
        chosen = jnp.concatenate([hits[0], hits[q + 1]], axis=1)
        out_ref[:, q * part : (q + 1) * part] = dot(chosen, rows).astype(BF)


def middle(heads, weight, residual, gain, routes, experts):
    tok, width = residual.shape
    return pl.pallas_call(
        middle_kernel,
        out_shape=(
            jax.ShapeDtypeStruct((tok, width), F32),
            jax.ShapeDtypeStruct((experts * ROWS, 3 * width // 4), BF),
        ),
        in_specs=vmem_specs(5),
        out_specs=tuple(vmem_specs(2)),
        compiler_params=pltpu.CompilerParams(vmem_limit_bytes=24 * MIB),
        name="middle",
    )(heads, weight, residual, gain, routes)


def moved(x, shift):
    return x if shift == 0 else pltpu.roll(x, shift, 1)


def by_source(x):
    rows, cols = x.shape
    x = x.reshape(rows // (4 * ROWS), 4, ROWS, cols)
    return [x[:, i] for i in range(4)]


def together(pieces):
    groups, rows, cols = pieces[0].shape
    return jnp.stack(pieces, axis=1).reshape(groups * len(pieces) * rows, cols)


def compacted(parts):
    found = [by_source(part.astype(F32)) for part in parts]
    row = lax.broadcasted_iota(jnp.int32, found[0][0].shape, 1)
    main = []
    for a, b, c, d in found:
        b, c, d = moved(b, 6), moved(c, 4), moved(d, 2)
        main.append(
            together(
                [jnp.where(row < 6, a, b), jnp.where(row < 4, b, c), jnp.where(row < 2, c, d)]
            ).astype(BF)
        )
    tails = []
    for tile in range(3):
        total = None
        for place in range(4):
            piece = 4 * tile + place
            x = moved(found[piece % 3][piece // 3], (2 * place + 2) % ROWS)
            total = x if total is None else jnp.where(row < 2 * place, total, x)
        tails.append(total)
    return main + [together(tails).astype(BF)]


def expanded(part, tail, q):
    rows, cols = part.shape
    x = part.reshape(rows // 24, 3, ROWS, cols)
    t = tail.reshape(rows // 24, 3, ROWS, cols)
    first, second, third = x[:, 0], x[:, 1], x[:, 2]
    row = lax.broadcasted_iota(jnp.int32, first.shape, 1)
    slots = [
        first,
        moved(jnp.where(row < 4, second, first), 2),
        moved(jnp.where(row < 2, third, second), 4),
        moved(third, 6),
    ]
    out = []
    for source in range(4):
        piece = 3 * source + q
        ends = moved(t[:, piece // 4], (6 - 2 * (piece % 4)) % ROWS)
        out.append(jnp.where(row < SLOTS, slots[source], ends))
    return together(out).astype(BF)


def experts_kernel(
    x_ref, gate_ref, up_ref, down_ref, routes_ref, weights_ref, out_ref, mix_ref, rows_ref, hidden_ref
):
    width, hidden = gate_ref.shape
    part = width // 4
    tile = 256
    blocks = compacted([x_ref[:, q * part : (q + 1) * part] for q in range(3)])
    for q in range(4):
        rows_ref[:, q * part : (q + 1) * part] = blocks[q]
    for g in range(hidden // tile):
        cols = slice(g * tile, (g + 1) * tile)
        gate = jnp.minimum(dot(rows_ref[...], gate_ref[:, cols]), 7.0)
        up = jnp.clip(dot(rows_ref[...], up_ref[:, cols]), -7.0, 7.0) + 1.0
        hidden_ref[:, cols] = (up * gate * jax.nn.sigmoid(1.702 * gate)).astype(BF)
    tail = dot(hidden_ref[...], down_ref[:, 3 * part :])
    for q in range(3):
        cols = slice(q * part, (q + 1) * part)
        out_ref[:, cols] = expanded(dot(hidden_ref[...], down_ref[:, cols]), tail, q)
    mix_table(routes_ref, weights_ref, mix_ref)


def experts(x, gate_weight, up_weight, down_weight, routes, weights):
    rows = x.shape[0]
    width, hidden = gate_weight.shape
    held = rows * SLOTS // ROWS
    return pl.pallas_call(
        experts_kernel,
        out_shape=(
            jax.ShapeDtypeStruct(x.shape, BF),
            pltpu.VMEM((8 * routes.shape[1], rows), BF),
        ),
        in_specs=vmem_specs(6),
        out_specs=tuple(vmem_specs(2)),
        scratch_shapes=[
            pltpu.VMEM((held, width), BF),
            pltpu.VMEM((held, hidden), BF),
        ],
        compiler_params=pltpu.CompilerParams(vmem_limit_bytes=30 * MIB),
        name="experts",
    )(x, gate_weight, up_weight, down_weight, routes, weights)


def combine_kernel(mixed_ref, rows_ref, mix_ref, out_ref):
    tok, width = mixed_ref.shape
    part = width // 4
    last = mixed_ref[:, 3 * part :]
    for q in range(3):
        cols = slice(q * part, (q + 1) * part)
        weights = jnp.concatenate(
            [mix_ref[0 : 2 * tok, :], mix_ref[(q + 1) * 2 * tok : (q + 2) * 2 * tok, :]], axis=0
        )
        sums = dot(weights, rows_ref[:, cols])
        out_ref[:, cols] = (mixed_ref[:, cols] + sums[0:tok] + sums[tok : 2 * tok]).astype(BF)
        last = last + sums[2 * tok : 3 * tok] + sums[3 * tok :]
    out_ref[:, 3 * part :] = last.astype(BF)


def combine(mixed, rows, mix):
    return pl.pallas_call(
        combine_kernel,
        out_shape=jax.ShapeDtypeStruct(mixed.shape, BF),
        in_specs=vmem_specs(3),
        out_specs=pl.BlockSpec(memory_space=pltpu.VMEM),
        compiler_params=pltpu.CompilerParams(vmem_limit_bytes=24 * MIB),
        name="combine",
    )(mixed, rows, mix)


def exchange(x, axis, devices):
    pieces = x.reshape(devices, x.shape[0] // devices, x.shape[1])
    out = lax.all_to_all(pieces, axis, split_axis=0, concat_axis=0, tiled=True)
    return out.reshape(x.shape)


def on_device(
    query_first,
    key_first,
    query_second,
    key_second,
    value_rows,
    mix_lambda,
    head_gain,
    residual,
    out_weight,
    norm_gain,
    routes,
    route_weights,
    gate_weight,
    up_weight,
    down_weight,
):
    along = lax.axis_size("sp")
    everyone = along * lax.axis_size("dp")
    packed = pack_heads(
        query_first[0], key_first[0], query_second[0], key_second[0], value_rows[0]
    )
    qkv = exchange(packed, "sp", along)
    chosen, shares = routes[0].T, route_weights[0].T
    head, weight, gates, ups, downs = attention(
        mix_lambda,
        head_gain.reshape(1, -1),
        qkv,
        out_weight,
        gate_weight[0],
        up_weight[0],
        down_weight[0],
    )
    heads = exchange(head, "sp", along)
    gain = norm_gain.reshape(1, -1)
    mixed, outgoing = middle(heads, weight, residual[0], gain, chosen, everyone)
    received = exchange(outgoing, ("sp", "dp"), everyone)
    finished, mix = experts(received, gates, ups, downs, chosen, shares)
    returned = exchange(finished, ("sp", "dp"), everyone)
    return combine(mixed, returned, mix)[None]


def solution(mesh):
    split = P("dp", "sp", None)
    held = P(("sp", "dp"), None, None)
    return jax.shard_map(
        on_device,
        mesh=mesh,
        in_specs=(split,) * 5 + (P(), P(), split, P(), P(), split, split) + (held,) * 3,
        out_specs=split,
        check_vma=False,
    )
```

time: 184 us -> 165 us (0.90)
  blocking collectives: 94.3 us -> 138 us
  waiting for transfers between devices: 30.3 us -> 0 us
  starting transfers between devices: 13.2 us -> 0 us
  local copies, waits for them, and re-layouts: 11 us -> 0.03 us
  Pallas kernels: 35 us -> 26.6 us
    all_to_all x2 -> x4, blocking collectives: 94.3 us -> 138 us  [exchange(): out = lax.all_to_all(pieces, axis, split_axis=0, concat_axis=0, tiled=True)]
    all_to_all x2 -> x0, waiting for transfers between devices: 30.3 us -> none  [exchange(): out = lax.all_to_all(pieces, axis, split_axis=0, concat_axis=0, tiled=True)]
    all_to_all x2 -> x0, starting transfers between devices: 13.2 us -> none  [exchange(): out = lax.all_to_all(pieces, axis, split_axis=0, concat_axis=0, tiled=True)]
    unnamed x30 -> x12, local copies, waits for them, and re-layouts: 10.5 us -> 0.03 us
    pallas_call x2 -> x1, Pallas kernels: 19.7 us -> 11.8 us  [experts(): pl.pallas_call(experts_kernel, out_shape=(jax.ShapeDtypeStruct(x.shape, B...]
  transfers between devices with their start and end apart: 2 -> 0, of which waited for: 2 -> 0; matrix products, arithmetic and copies ran while one was open for 0% -> 0% of each run, Pallas kernels for 1% -> 0%
where the time goes in v1:
time: 165 us; the launch traced here: 164 us
  blocking collectives  138 us (84%)
  Pallas kernels  26.6 us (16%)
    all_to_all x4, blocking collectives, exchange(): out = lax.all_to_all(pieces, axis, split_axis=0, concat_axis=0, tiled=True)  138 us
    pallas_call x1, Pallas kernels, experts(): pl.pallas_call(experts_kernel, out_shape=(jax.ShapeDtypeStruct(x.shape, B...  11.8 us
    pallas_call x1, Pallas kernels, attention(): pl.pallas_call(functools.partial(attention_kernel, block=256), out_shape=...  8.2 us

profile of v1, /device:TPU:1, one launch (start us, length us, event | category | flops | bytes accessed | tf_op | source)
XLA Modules:
  0.0 164.4 jit_solution(13315855491923705805)
XLA Ops:
  0.0 0.0 copy-start.5
  0.0 0.0 copy-start.4
  0.0 1.6 pack_heads.1
  1.6 30.0 %all_to_all.20 = bf16[16,128,384]{2,1,0:T(8,128)(2,1)S(1)} all-to-all(bf16[16,128,384]{2,1,0:T(8,128)(2,1)S(1)} %bitcast.29), channel_id=1, replica_groups=mesh['sp'=16,'dp'=8] {'sp'}, dimensions={0} | all-to-all | bytes 3145728 | tf_op jit(solution)/shard_map/all_to_all | solution.py:354
  31.7 0.0 copy-done.5
  31.7 0.0 copy-done.4
  31.7 0.0 copy-start
  31.7 0.0 copy-start.1
  31.7 0.0 copy-start.2
  31.7 8.2 %attention.1 = (bf16[2048,128]{1,0:T(8,128)(2,1)S(1)}, bf16[2048,2048]{1,0:T(8,128)(2,1)S(1)}, bf16[2048,1024]{1,0:T(8,128)(2,1)S(1)}, bf16[2048,1024]{1,0:T(8,128)(2,1)S(1)}, bf16[1024,2048]{1,0:T(8,128)(2,1)S(1)}) custom-call(f32[16]{0:T(128)S(1)} %copy-done.4, f32[1,128]{1,0:T(1,128)S(1)} %bitcast.39, bf16[2048,384]{1,0:T(8,128)(2,1)S(1)} %bitcast.28, ...), custom_call_target="tpu_custom_call" | custom-call | tf_op jit(solution)/shard_map/attention/pallas_call | solution.py:123
  39.9 13.3 %all_to_all.21 = bf16[16,128,128]{2,1,0:T(8,128)(2,1)S(1)} all-to-all(bf16[16,128,128]{2,1,0:T(8,128)(2,1)S(1)} %bitcast.34), channel_id=1, replica_groups=mesh['sp'=16,'dp'=8] {'sp'}, dimensions={0} | all-to-all | bytes 1048576 | tf_op jit(solution)/shard_map/all_to_all | solution.py:354
  53.2 0.0 copy-done
  53.2 0.0 copy-done.1
  53.2 0.0 copy-done.2
  53.2 2.4 %middle.1 = (f32[128,2048]{1,0:T(8,128)S(1)}, bf16[1024,1536]{1,0:T(8,128)(2,1)S(1)}) custom-call(bf16[2048,128]{1,0:T(8,128)(2,1)S(1)} %bitcast.32, bf16[2048,2048]{1,0:T(8,128)(2,1)S(1)} %get-tuple-element.15.weight_ref, bf16[128,2048]{1,0:T(8,128)(2,1)S(1)} %bitcast.33, f32[1,2048]{1,0:T(1,128)S(1)} %bitcast.37, s32[4,128]{1,0:T(4,128)S(1)} %bitcast.35), custom_call_target="tpu_custom_call" | custom-call | tf_op jit(solution)/shard_map/middle/pallas_call | solution.py:214
  55.7 0.0 copy-start.3
  55.7 48.8 %all_to_all.22 = bf16[128,8,1536]{2,1,0:T(8,128)(2,1)S(1)} all-to-all(bf16[128,8,1536]{2,1,0:T(8,128)(2,1)S(1)} %bitcast.31), channel_id=1, replica_groups=mesh['sp'=16,'dp'=8] {'sp','dp'}, dimensions={0} | all-to-all | bytes 6291456 | tf_op jit(solution)/shard_map/all_to_all | solution.py:354
  104.5 0.0 copy-done.3
  104.5 11.8 %experts.1 = (bf16[1024,1536]{1,0:T(8,128)(2,1)S(1)}, bf16[1024,1024]{1,0:T(8,128)(2,1)S(1)}) custom-call(bf16[1024,1536]{1,0:T(8,128)(2,1)S(1)} %bitcast.26, bf16[2048,1024]{1,0:T(8,128)(2,1)S(1)} %get-tuple-element.18.gate_ref, bf16[2048,1024]{1,0:T(8,128)(2,1)S(1)} %get-tuple-element.19.up_ref, bf16[1024,2048]{1,0:T(8,128)(2,1)S(1)} %get-tuple-element.20.down_ref, ...), custom_call_target="tpu_custom_call" | custom-call | tf_op jit(solution)/shard_map/experts/pallas_call | solution.py:309
  116.2 45.6 %all_to_all.23 = bf16[128,8,1536]{2,1,0:T(8,128)(2,1)S(1)} all-to-all(bf16[128,8,1536]{2,1,0:T(8,128)(2,1)S(1)} %bitcast.30), channel_id=1, replica_groups=mesh['sp'=16,'dp'=8] {'sp','dp'}, dimensions={0} | all-to-all | bytes 6291456 | tf_op jit(solution)/shard_map/all_to_all | solution.py:354
  161.8 2.6 %combine.1 = bf16[128,2048]{1,0:T(8,128)(2,1)} custom-call(f32[128,2048]{1,0:T(8,128)S(1)} %get-tuple-element.16.mixed_ref, bf16[1024,1536]{1,0:T(8,128)(2,1)S(1)} %bitcast.27, bf16[1024,1024]{1,0:T(8,128)(2,1)S(1)} %get-tuple-element.22.mix_ref), custom_call_target="tpu_custom_call" | custom-call | tf_op jit(solution)/shard_map/combine/pallas_call | solution.py:342
Async XLA Ops:
  0.0 31.7 %copy-start.5 = (f32[128]{0:T(128)S(1)}, f32[128]{0:T(128)}, u32[]{:S(2)}) copy-start(f32[128]{0:T(128)} %param.21) | copy-start | bytes 1540
  0.0 31.7 %copy-start.4 = (f32[16]{0:T(128)S(1)}, f32[16]{0:T(128)}, u32[]{:S(2)}) copy-start(f32[16]{0:T(128)} %lam_ref.1) | copy-start | bytes 196
  31.7 21.6 %copy-start = (bf16[1,128,2048]{2,1,0:T(8,128)(2,1)S(1)}, bf16[1,128,2048]{2,1,0:T(8,128)(2,1)}, u32[]{:S(2)}) copy-start(bf16[1,128,2048]{2,1,0:T(8,128)(2,1)} %param.22) | copy-start | bytes 1572868
  31.7 21.6 %copy-start.1 = (s32[1,128,4]{1,2,0:T(4,128)S(1)}, s32[1,128,4]{1,2,0:T(4,128)}, u32[]{:S(2)}) copy-start(s32[1,128,4]{1,2,0:T(4,128)} %param.25) | copy-start | bytes 6148
  31.7 21.5 %copy-start.2 = (f32[2048]{0:T(1024)S(1)}, f32[2048]{0:T(1024)}, u32[]{:S(2)}) copy-start(f32[2048]{0:T(1024)} %param.24) | copy-start | bytes 24580
  55.7 48.8 %copy-start.3 = (f32[1,128,4]{1,2,0:T(4,128)S(1)}, f32[1,128,4]{1,2,0:T(4,128)}, u32[]{:S(2)}) copy-start(f32[1,128,4]{1,2,0:T(4,128)} %param.26) | copy-start | bytes 6148

commit v2 on v1

--- a/solution.py
+++ b/solution.py
@@ -85,32 +85,37 @@
     )
     lam = lam_ref[lax.axis_index("sp")]
     gain = gain_ref[...]
-    for step in range(length // block):
-        rows = slice(step * block, (step + 1) * block)
-        queries = qkv_ref[rows, 0:LANES]
+    steps = length // block
+    ones = jnp.ones((block, LANES), BF)
+
+    def both_maps(step):
+        queries = qkv_ref[step * block : (step + 1) * block, 0:LANES]
         zero = jnp.zeros_like(queries)
-        both = jnp.concatenate(
+        return jnp.concatenate(
             [jnp.where(lane < half, queries, zero), jnp.where(lane < half, zero, queries)], axis=0
         )
-        scores = []
-        for c in range(step + 1):
-            keys = qkv_ref[c * block : (c + 1) * block, LANES : 2 * LANES]
-            s = dot(both, keys, ((1,), (1,)))
-            if c == step:
-                s = jnp.where(causal, s, -1e30)
-            scores.append(s)
-        top = functools.reduce(jnp.maximum, scores)
-        top = jnp.max(top, axis=1, keepdims=True)
-        total = None
+
+    def score(both, step, c):
+        s = dot(both, qkv_ref[c * block : (c + 1) * block, LANES : 2 * LANES], ((1,), (1,)))
+        return jnp.where(causal, s, -1e30) if c == step else s
+
+    following = [score(both_maps(0), 0, 0)]
+    for step in range(steps):
+        rows = slice(step * block, (step + 1) * block)
+        scores, following = following, []
+        top = jnp.max(functools.reduce(jnp.maximum, scores), axis=1, keepdims=True)
+        both = both_maps(step + 1) if step + 1 < steps else None
         raw = None
-        for c in range(step + 1):
-            p = jnp.exp2((scores[c] - top) * scale)
-            total = p if total is None else total + p
-            values = qkv_ref[c * block : (c + 1) * block, 2 * LANES : 3 * LANES]
-            part = dot(p.astype(BF), values)
-            raw = part if raw is None else raw + part
-        total = jnp.sum(total, axis=1, keepdims=True)
-        normal = raw / total
+        probs = []
+        for c in range(step + 2):
+            if both is not None:
+                following.append(score(both, step + 1, c))
+            if c <= step:
+                p = jnp.exp2((scores[c] - top) * scale).astype(BF)
+                values = qkv_ref[c * block : (c + 1) * block, 2 * LANES : 3 * LANES]
+                part = dot(p, jnp.concatenate([values, ones], axis=1))
+                raw = part if raw is None else raw + part
+        normal = raw[:, :LANES] / raw[:, LANES : LANES + 1]
         head = normal[:block] - lam * normal[block:]
         factor = lax.rsqrt(jnp.mean(head * head, axis=1, keepdims=True) + 1e-06)
         out_ref[rows, :] = (head * factor * gain).astype(BF)
@@ -172,13 +177,9 @@
     weight = jnp.zeros(slot.shape, F32)
     for k, hit in enumerate(hits):
         weight = jnp.where(hit, weights_ref[k : k + 1, :], weight)
-    high = weight.astype(BF).astype(F32)
-    low = spread(weight - high)
-    high = spread(high)
+    weight = spread(weight)
     for part, hit in enumerate(slot_hits(slot)):
-        base = part * 2 * tok
-        mix_ref[base : base + tok, :] = jnp.where(hit, high, 0.0).T.astype(BF)
-        mix_ref[base + tok : base + 2 * tok, :] = jnp.where(hit, low, 0.0).T.astype(BF)
+        mix_ref[part * tok : (part + 1) * tok, :] = jnp.where(hit, weight, 0.0).T.astype(BF)
 
 
 def middle_kernel(
@@ -310,7 +311,7 @@
         experts_kernel,
         out_shape=(
             jax.ShapeDtypeStruct(x.shape, BF),
-            pltpu.VMEM((8 * routes.shape[1], rows), BF),
+            pltpu.VMEM((4 * routes.shape[1], rows), BF),
         ),
         in_specs=vmem_specs(6),
         out_specs=tuple(vmem_specs(2)),
@@ -330,11 +331,11 @@
     for q in range(3):
         cols = slice(q * part, (q + 1) * part)
         weights = jnp.concatenate(
-            [mix_ref[0 : 2 * tok, :], mix_ref[(q + 1) * 2 * tok : (q + 2) * 2 * tok, :]], axis=0
+            [mix_ref[0:tok, :], mix_ref[(q + 1) * tok : (q + 2) * tok, :]], axis=0
         )
         sums = dot(weights, rows_ref[:, cols])
-        out_ref[:, cols] = (mixed_ref[:, cols] + sums[0:tok] + sums[tok : 2 * tok]).astype(BF)
-        last = last + sums[2 * tok : 3 * tok] + sums[3 * tok :]
+        out_ref[:, cols] = (mixed_ref[:, cols] + sums[:tok]).astype(BF)
+        last = last + sums[tok:]
     out_ref[:, 3 * part :] = last.astype(BF)
 
 

time: 165 us -> 163 us (0.988)
  Pallas kernels: 26.6 us -> 24.7 us
where the time goes in v2:
time: 163 us
  blocking collectives  138 us (85%)
  Pallas kernels  24.7 us (15%)
    all_to_all x4, blocking collectives, exchange(): out = lax.all_to_all(pieces, axis, split_axis=0, concat_axis=0, tiled=True)  138 us
    pallas_call x1, Pallas kernels, experts(): pl.pallas_call(experts_kernel, out_shape=(jax.ShapeDtypeStruct(x.shape, B...  11.3 us
    pallas_call x1, Pallas kernels, attention(): pl.pallas_call(functools.partial(attention_kernel, block=256), out_shape=...  7.56 us

profile of v2, /device:TPU:1, one launch (start us, length us, event | category | flops | bytes accessed | tf_op | source)
XLA Modules:
  0.0 162.6 jit_solution(1650041876485757789)
XLA Ops:
  0.0 0.0 copy-start.5
  0.0 0.0 copy-start.4
  0.0 1.6 pack_heads.1
  1.6 30.0 %all_to_all.20 = bf16[16,128,384]{2,1,0:T(8,128)(2,1)S(1)} all-to-all(bf16[16,128,384]{2,1,0:T(8,128)(2,1)S(1)} %bitcast.29), channel_id=1, replica_groups=mesh['sp'=16,'dp'=8] {'sp'}, dimensions={0} | all-to-all | bytes 3145728 | tf_op jit(solution)/shard_map/all_to_all | solution.py:355
  31.7 0.0 copy-done.5
  31.7 0.0 copy-done.4
  31.7 0.0 copy-start
  31.7 0.0 copy-start.1
  31.7 0.0 copy-start.2
  31.7 7.6 %attention.1 = (bf16[2048,128]{1,0:T(8,128)(2,1)S(1)}, bf16[2048,2048]{1,0:T(8,128)(2,1)S(1)}, bf16[2048,1024]{1,0:T(8,128)(2,1)S(1)}, bf16[2048,1024]{1,0:T(8,128)(2,1)S(1)}, bf16[1024,2048]{1,0:T(8,128)(2,1)S(1)}) custom-call(f32[16]{0:T(128)S(1)} %copy-done.4, f32[1,128]{1,0:T(1,128)S(1)} %bitcast.39, bf16[2048,384]{1,0:T(8,128)(2,1)S(1)} %bitcast.28, ...), custom_call_target="tpu_custom_call" | custom-call | tf_op jit(solution)/shard_map/attention/pallas_call | solution.py:128
  39.3 13.3 %all_to_all.21 = bf16[16,128,128]{2,1,0:T(8,128)(2,1)S(1)} all-to-all(bf16[16,128,128]{2,1,0:T(8,128)(2,1)S(1)} %bitcast.34), channel_id=1, replica_groups=mesh['sp'=16,'dp'=8] {'sp'}, dimensions={0} | all-to-all | bytes 1048576 | tf_op jit(solution)/shard_map/all_to_all | solution.py:355
  52.6 0.0 copy-done
  52.6 0.0 copy-done.1
  52.6 0.0 copy-done.2
  52.6 2.4 %middle.1 = (f32[128,2048]{1,0:T(8,128)S(1)}, bf16[1024,1536]{1,0:T(8,128)(2,1)S(1)}) custom-call(bf16[2048,128]{1,0:T(8,128)(2,1)S(1)} %bitcast.32, bf16[2048,2048]{1,0:T(8,128)(2,1)S(1)} %get-tuple-element.15.weight_ref, bf16[128,2048]{1,0:T(8,128)(2,1)S(1)} %bitcast.33, f32[1,2048]{1,0:T(1,128)S(1)} %bitcast.37, s32[4,128]{1,0:T(4,128)S(1)} %bitcast.35), custom_call_target="tpu_custom_call" | custom-call | tf_op jit(solution)/shard_map/middle/pallas_call | solution.py:215
  55.0 0.0 copy-start.3
  55.0 48.8 %all_to_all.22 = bf16[128,8,1536]{2,1,0:T(8,128)(2,1)S(1)} all-to-all(bf16[128,8,1536]{2,1,0:T(8,128)(2,1)S(1)} %bitcast.31), channel_id=1, replica_groups=mesh['sp'=16,'dp'=8] {'sp','dp'}, dimensions={0} | all-to-all | bytes 6291456 | tf_op jit(solution)/shard_map/all_to_all | solution.py:355
  103.8 0.0 copy-done.3
  103.9 11.3 %experts.1 = (bf16[1024,1536]{1,0:T(8,128)(2,1)S(1)}, bf16[512,1024]{1,0:T(8,128)(2,1)S(1)}) custom-call(bf16[1024,1536]{1,0:T(8,128)(2,1)S(1)} %bitcast.26, bf16[2048,1024]{1,0:T(8,128)(2,1)S(1)} %get-tuple-element.18.gate_ref, bf16[2048,1024]{1,0:T(8,128)(2,1)S(1)} %get-tuple-element.19.up_ref, bf16[1024,2048]{1,0:T(8,128)(2,1)S(1)} %get-tuple-element.20.down_ref, ...), custom_call_target="tpu_custom_call" | custom-call | tf_op jit(solution)/shard_map/experts/pallas_call | solution.py:310
  115.2 45.6 %all_to_all.23 = bf16[128,8,1536]{2,1,0:T(8,128)(2,1)S(1)} all-to-all(bf16[128,8,1536]{2,1,0:T(8,128)(2,1)S(1)} %bitcast.30), channel_id=1, replica_groups=mesh['sp'=16,'dp'=8] {'sp','dp'}, dimensions={0} | all-to-all | bytes 6291456 | tf_op jit(solution)/shard_map/all_to_all | solution.py:355
  160.8 1.8 %combine.1 = bf16[128,2048]{1,0:T(8,128)(2,1)} custom-call(f32[128,2048]{1,0:T(8,128)S(1)} %get-tuple-element.16.mixed_ref, bf16[1024,1536]{1,0:T(8,128)(2,1)S(1)} %bitcast.27, bf16[512,1024]{1,0:T(8,128)(2,1)S(1)} %get-tuple-element.22.mix_ref), custom_call_target="tpu_custom_call" | custom-call | tf_op jit(solution)/shard_map/combine/pallas_call | solution.py:343
Async XLA Ops:
  0.0 31.7 %copy-start.5 = (f32[128]{0:T(128)S(1)}, f32[128]{0:T(128)}, u32[]{:S(2)}) copy-start(f32[128]{0:T(128)} %param.21) | copy-start | bytes 1540
  0.0 31.7 %copy-start.4 = (f32[16]{0:T(128)S(1)}, f32[16]{0:T(128)}, u32[]{:S(2)}) copy-start(f32[16]{0:T(128)} %lam_ref.1) | copy-start | bytes 196
  31.7 20.9 %copy-start = (bf16[1,128,2048]{2,1,0:T(8,128)(2,1)S(1)}, bf16[1,128,2048]{2,1,0:T(8,128)(2,1)}, u32[]{:S(2)}) copy-start(bf16[1,128,2048]{2,1,0:T(8,128)(2,1)} %param.22) | copy-start | bytes 1572868
  31.7 20.9 %copy-start.1 = (s32[1,128,4]{1,2,0:T(4,128)S(1)}, s32[1,128,4]{1,2,0:T(4,128)}, u32[]{:S(2)}) copy-start(s32[1,128,4]{1,2,0:T(4,128)} %param.25) | copy-start | bytes 6148
  31.7 20.9 %copy-start.2 = (f32[2048]{0:T(1024)S(1)}, f32[2048]{0:T(1024)}, u32[]{:S(2)}) copy-start(f32[2048]{0:T(1024)} %param.24) | copy-start | bytes 24580
  55.0 48.8 %copy-start.3 = (f32[1,128,4]{1,2,0:T(4,128)S(1)}, f32[1,128,4]{1,2,0:T(4,128)}, u32[]{:S(2)}) copy-start(f32[1,128,4]{1,2,0:T(4,128)} %param.26) | copy-start | bytes 6148

commit v3 on v2

--- a/solution.py
+++ b/solution.py
@@ -324,9 +324,13 @@
     )(x, gate_weight, up_weight, down_weight, routes, weights)
 
 
-def combine_kernel(mixed_ref, rows_ref, mix_ref, out_ref):
+def combine_kernel(mixed_ref, rows_ref, mix_ref, out_hbm, out_ref, sems):
     tok, width = mixed_ref.shape
     part = width // 4
+    copies = []
+    for q in range(4):
+        cols = slice(q * part, (q + 1) * part)
+        copies.append(pltpu.make_async_copy(out_ref.at[:, cols], out_hbm.at[:, cols], sems.at[q]))
     last = mixed_ref[:, 3 * part :]
     for q in range(3):
         cols = slice(q * part, (q + 1) * part)
@@ -335,8 +339,12 @@
         )
         sums = dot(weights, rows_ref[:, cols])
         out_ref[:, cols] = (mixed_ref[:, cols] + sums[:tok]).astype(BF)
+        copies[q].start()
         last = last + sums[tok:]
     out_ref[:, 3 * part :] = last.astype(BF)
+    copies[3].start()
+    for copy in copies:
+        copy.wait()
 
 
 def combine(mixed, rows, mix):
@@ -344,7 +352,8 @@
         combine_kernel,
         out_shape=jax.ShapeDtypeStruct(mixed.shape, BF),
         in_specs=vmem_specs(3),
-        out_specs=pl.BlockSpec(memory_space=pltpu.VMEM),
+        out_specs=pl.BlockSpec(memory_space=pltpu.HBM),
+        scratch_shapes=[pltpu.VMEM(mixed.shape, BF), pltpu.SemaphoreType.DMA((4,))],
         compiler_params=pltpu.CompilerParams(vmem_limit_bytes=24 * MIB),
         name="combine",
     )(mixed, rows, mix)

time: 163 us -> 163 us (level)
  no operation moved by 1% of the time
where the time goes in v3:
time: 163 us
  blocking collectives  138 us (85%)
  Pallas kernels  24.6 us (15%)
    all_to_all x4, blocking collectives, exchange(): out = lax.all_to_all(pieces, axis, split_axis=0, concat_axis=0, tiled=True)  138 us
    pallas_call x1, Pallas kernels, experts(): pl.pallas_call(experts_kernel, out_shape=(jax.ShapeDtypeStruct(x.shape, B...  11.3 us
    pallas_call x1, Pallas kernels, attention(): pl.pallas_call(functools.partial(attention_kernel, block=256), out_shape=...  7.56 us

profile of v3, /device:TPU:1, one launch (start us, length us, event | category | flops | bytes accessed | tf_op | source)
XLA Modules:
  0.0 162.7 jit_solution(5198344790567026181)
XLA Ops:
  0.0 0.0 copy-start.5
  0.0 0.0 copy-start.4
  0.0 1.6 pack_heads.1
  1.6 30.0 %all_to_all.20 = bf16[16,128,384]{2,1,0:T(8,128)(2,1)S(1)} all-to-all(bf16[16,128,384]{2,1,0:T(8,128)(2,1)S(1)} %bitcast.29), channel_id=1, replica_groups=mesh['sp'=16,'dp'=8] {'sp'}, dimensions={0} | all-to-all | bytes 3145728 | tf_op jit(solution)/shard_map/all_to_all | solution.py:364
  31.7 0.0 copy-done.5
  31.7 0.0 copy-done.4
  31.7 0.0 copy-start
  31.7 0.0 copy-start.1
  31.7 0.0 copy-start.2
  31.7 7.6 %attention.1 = (bf16[2048,128]{1,0:T(8,128)(2,1)S(1)}, bf16[2048,2048]{1,0:T(8,128)(2,1)S(1)}, bf16[2048,1024]{1,0:T(8,128)(2,1)S(1)}, bf16[2048,1024]{1,0:T(8,128)(2,1)S(1)}, bf16[1024,2048]{1,0:T(8,128)(2,1)S(1)}) custom-call(f32[16]{0:T(128)S(1)} %copy-done.4, f32[1,128]{1,0:T(1,128)S(1)} %bitcast.39, bf16[2048,384]{1,0:T(8,128)(2,1)S(1)} %bitcast.28, ...), custom_call_target="tpu_custom_call" | custom-call | tf_op jit(solution)/shard_map/attention/pallas_call | solution.py:128
  39.3 13.3 %all_to_all.21 = bf16[16,128,128]{2,1,0:T(8,128)(2,1)S(1)} all-to-all(bf16[16,128,128]{2,1,0:T(8,128)(2,1)S(1)} %bitcast.34), channel_id=1, replica_groups=mesh['sp'=16,'dp'=8] {'sp'}, dimensions={0} | all-to-all | bytes 1048576 | tf_op jit(solution)/shard_map/all_to_all | solution.py:364
  52.6 0.0 copy-done
  52.6 0.0 copy-done.1
  52.6 0.0 copy-done.2
  52.6 2.4 %middle.1 = (f32[128,2048]{1,0:T(8,128)S(1)}, bf16[1024,1536]{1,0:T(8,128)(2,1)S(1)}) custom-call(bf16[2048,128]{1,0:T(8,128)(2,1)S(1)} %bitcast.32, bf16[2048,2048]{1,0:T(8,128)(2,1)S(1)} %get-tuple-element.15.weight_ref, bf16[128,2048]{1,0:T(8,128)(2,1)S(1)} %bitcast.33, f32[1,2048]{1,0:T(1,128)S(1)} %bitcast.37, s32[4,128]{1,0:T(4,128)S(1)} %bitcast.35), custom_call_target="tpu_custom_call" | custom-call | tf_op jit(solution)/shard_map/middle/pallas_call | solution.py:215
  55.0 0.0 copy-start.3
  55.0 48.8 %all_to_all.22 = bf16[128,8,1536]{2,1,0:T(8,128)(2,1)S(1)} all-to-all(bf16[128,8,1536]{2,1,0:T(8,128)(2,1)S(1)} %bitcast.31), channel_id=1, replica_groups=mesh['sp'=16,'dp'=8] {'sp','dp'}, dimensions={0} | all-to-all | bytes 6291456 | tf_op jit(solution)/shard_map/all_to_all | solution.py:364
  103.8 0.0 copy-done.3
  103.9 11.3 %experts.1 = (bf16[1024,1536]{1,0:T(8,128)(2,1)S(1)}, bf16[512,1024]{1,0:T(8,128)(2,1)S(1)}) custom-call(bf16[1024,1536]{1,0:T(8,128)(2,1)S(1)} %bitcast.26, bf16[2048,1024]{1,0:T(8,128)(2,1)S(1)} %get-tuple-element.18.gate_ref, bf16[2048,1024]{1,0:T(8,128)(2,1)S(1)} %get-tuple-element.19.up_ref, bf16[1024,2048]{1,0:T(8,128)(2,1)S(1)} %get-tuple-element.20.down_ref, ...), custom_call_target="tpu_custom_call" | custom-call | tf_op jit(solution)/shard_map/experts/pallas_call | solution.py:310
  115.2 45.6 %all_to_all.23 = bf16[128,8,1536]{2,1,0:T(8,128)(2,1)S(1)} all-to-all(bf16[128,8,1536]{2,1,0:T(8,128)(2,1)S(1)} %bitcast.30), channel_id=1, replica_groups=mesh['sp'=16,'dp'=8] {'sp','dp'}, dimensions={0} | all-to-all | bytes 6291456 | tf_op jit(solution)/shard_map/all_to_all | solution.py:364
  160.8 1.7 %combine.1 = bf16[128,2048]{1,0:T(8,128)(2,1)} custom-call(f32[128,2048]{1,0:T(8,128)S(1)} %get-tuple-element.16.mixed_ref, bf16[1024,1536]{1,0:T(8,128)(2,1)S(1)} %bitcast.27, bf16[512,1024]{1,0:T(8,128)(2,1)S(1)} %get-tuple-element.22.mix_ref), custom_call_target="tpu_custom_call" | custom-call | tf_op jit(solution)/shard_map/combine/pallas_call | solution.py:351
Async XLA Ops:
  0.0 31.7 %copy-start.5 = (f32[128]{0:T(128)S(1)}, f32[128]{0:T(128)}, u32[]{:S(2)}) copy-start(f32[128]{0:T(128)} %param.21) | copy-start | bytes 1540
  0.0 31.7 %copy-start.4 = (f32[16]{0:T(128)S(1)}, f32[16]{0:T(128)}, u32[]{:S(2)}) copy-start(f32[16]{0:T(128)} %lam_ref.1) | copy-start | bytes 196
  31.7 20.9 %copy-start = (bf16[1,128,2048]{2,1,0:T(8,128)(2,1)S(1)}, bf16[1,128,2048]{2,1,0:T(8,128)(2,1)}, u32[]{:S(2)}) copy-start(bf16[1,128,2048]{2,1,0:T(8,128)(2,1)} %param.22) | copy-start | bytes 1572868
  31.7 20.9 %copy-start.1 = (s32[1,128,4]{1,2,0:T(4,128)S(1)}, s32[1,128,4]{1,2,0:T(4,128)}, u32[]{:S(2)}) copy-start(s32[1,128,4]{1,2,0:T(4,128)} %param.25) | copy-start | bytes 6148
  31.7 20.9 %copy-start.2 = (f32[2048]{0:T(1024)S(1)}, f32[2048]{0:T(1024)}, u32[]{:S(2)}) copy-start(f32[2048]{0:T(1024)} %param.24) | copy-start | bytes 24580
  55.0 48.8 %copy-start.3 = (f32[1,128,4]{1,2,0:T(4,128)S(1)}, f32[1,128,4]{1,2,0:T(4,128)}, u32[]{:S(2)}) copy-start(f32[1,128,4]{1,2,0:T(4,128)} %param.26) | copy-start | bytes 6148

commit v4 on v2

--- a/solution.py
+++ b/solution.py
@@ -69,8 +69,8 @@
 def attention_kernel(
     lam_ref, gain_ref, qkv_ref, *refs, block
 ):
-    held = (len(refs) - 2) // 2
-    out_ref, sems = refs[held], refs[-1]
+    held = (len(refs) - 3) // 2
+    out_ref, flat_ref, sems = refs[held], refs[-2], refs[-1]
     loads = [
         pltpu.make_async_copy(refs[i], refs[held + 1 + i], sems.at[i]) for i in range(held)
     ]
@@ -80,13 +80,16 @@
     half = LANES // 2
     scale = (half**-0.5) * 1.4426950408889634
     lane = lax.broadcasted_iota(jnp.int32, (block, LANES), 1)
-    causal = lax.broadcasted_iota(jnp.int32, (2 * block, block), 1) <= (
-        lax.broadcasted_iota(jnp.int32, (2 * block, block), 0) & (block - 1)
+    causal = lax.broadcasted_iota(jnp.int32, (block, 2 * block), 0) <= (
+        lax.broadcasted_iota(jnp.int32, (block, 2 * block), 1) & (block - 1)
     )
     lam = lam_ref[lax.axis_index("sp")]
     gain = gain_ref[...]
     steps = length // block
-    ones = jnp.ones((block, LANES), BF)
+    for c in range(steps):
+        keys = slice(c * block, (c + 1) * block)
+        flat_ref[0:LANES, keys] = qkv_ref[keys, 2 * LANES : 3 * LANES].T
+    flat_ref[LANES:, :] = jnp.ones((flat_ref.shape[0] - LANES, length), BF)
 
     def both_maps(step):
         queries = qkv_ref[step * block : (step + 1) * block, 0:LANES]
@@ -95,30 +98,47 @@
             [jnp.where(lane < half, queries, zero), jnp.where(lane < half, zero, queries)], axis=0
         )
 
-    def score(both, step, c):
-        s = dot(both, qkv_ref[c * block : (c + 1) * block, LANES : 2 * LANES], ((1,), (1,)))
-        return jnp.where(causal, s, -1e30) if c == step else s
-
-    following = [score(both_maps(0), 0, 0)]
-    for step in range(steps):
-        rows = slice(step * block, (step + 1) * block)
+    wide = 2 * block
+
+    def pair_maps(pair):
+        return jnp.concatenate([both_maps(2 * pair), both_maps(2 * pair + 1)], axis=0)
+
+    def score(both, pair, c):
+        keys = qkv_ref[c * block : (c + 1) * block, LANES : 2 * LANES]
+        if c > 2 * pair:
+            return jnp.where(causal, dot(keys, both[wide:], ((1,), (1,))), -1e30)
+        s = dot(keys, both, ((1,), (1,)))
+        if c == 2 * pair:
+            s = jnp.concatenate([jnp.where(causal, s[:, :wide], -1e30), s[:, wide:]], axis=1)
+        return s
+
+    pairs = steps // 2
+    both = pair_maps(0)
+    following = [score(both, 0, 0), score(both, 0, 1)]
+    for pair in range(pairs):
         scores, following = following, []
-        top = jnp.max(functools.reduce(jnp.maximum, scores), axis=1, keepdims=True)
-        both = both_maps(step + 1) if step + 1 < steps else None
+        top = jnp.max(functools.reduce(jnp.maximum, scores[:-1]), axis=0, keepdims=True)
+        late = jnp.maximum(top[:, wide:], jnp.max(scores[-1], axis=0, keepdims=True))
+        top = jnp.concatenate([top[:, :wide], late], axis=1)
+        both = pair_maps(pair + 1) if pair + 1 < pairs else None
         raw = None
-        probs = []
-        for c in range(step + 2):
+        for c in range(2 * pair + 4):
             if both is not None:
-                following.append(score(both, step + 1, c))
-            if c <= step:
-                p = jnp.exp2((scores[c] - top) * scale).astype(BF)
-                values = qkv_ref[c * block : (c + 1) * block, 2 * LANES : 3 * LANES]
-                part = dot(p, jnp.concatenate([values, ones], axis=1))
-                raw = part if raw is None else raw + part
-        normal = raw[:, :LANES] / raw[:, LANES : LANES + 1]
-        head = normal[:block] - lam * normal[block:]
-        factor = lax.rsqrt(jnp.mean(head * head, axis=1, keepdims=True) + 1e-06)
-        out_ref[rows, :] = (head * factor * gain).astype(BF)
+                following.append(score(both, pair + 1, c))
+            if c < 2 * pair + 2:
+                last = c == 2 * pair + 1
+                p = jnp.exp2((scores[c] - (late if last else top)) * scale).astype(BF)
+                part = dot(flat_ref[:, c * block : (c + 1) * block], p)
+                if last:
+                    raw = (raw[:, :wide], raw[:, wide:] + part)
+                else:
+                    raw = part if raw is None else raw + part
+        for i in range(2):
+            begin = (2 * pair + i) * block
+            normal = raw[i][:LANES] / raw[i][LANES : LANES + 1]
+            head = normal[:, :block] - lam * normal[:, block:]
+            factor = lax.rsqrt(jnp.mean(head * head, axis=0, keepdims=True) + 1e-06)
+            out_ref[begin : begin + block, :] = ((head * factor).T * gain).astype(BF)
     for load in loads:
         load.wait()
 
@@ -133,7 +153,10 @@
         + vmem_specs(2)
         + [pl.BlockSpec(memory_space=pltpu.HBM)] * len(weights),
         out_specs=tuple(vmem_specs(1 + len(weights))),
-        scratch_shapes=[pltpu.SemaphoreType.DMA((len(weights),))],
+        scratch_shapes=[
+            pltpu.VMEM((LANES + 16, length), BF),
+            pltpu.SemaphoreType.DMA((len(weights),)),
+        ],
         compiler_params=pltpu.CompilerParams(vmem_limit_bytes=24 * MIB),
         name="attention",
     )(lam, gain, qkv, *in_hbm(*weights))

time: 163 us -> 163 us (level)
  no operation moved by 1% of the time
where the time goes in v4:
time: 163 us
  blocking collectives  138 us (85%)
  Pallas kernels  24.7 us (15%)
    all_to_all x4, blocking collectives, exchange(): out = lax.all_to_all(pieces, axis, split_axis=0, concat_axis=0, tiled=True)  138 us
    pallas_call x1, Pallas kernels, experts(): pl.pallas_call(experts_kernel, out_shape=(jax.ShapeDtypeStruct(x.shape, B...  11.3 us
    pallas_call x1, Pallas kernels, attention(): pl.pallas_call(functools.partial(attention_kernel, block=256), out_shape=...  7.56 us

profile of v4, /device:TPU:1, one launch (start us, length us, event | category | flops | bytes accessed | tf_op | source)
XLA Modules:
  0.0 162.6 jit_solution(3857866759883184629)
XLA Ops:
  0.0 0.0 copy-start.5
  0.0 0.0 copy-start.4
  0.0 1.6 pack_heads.1
  1.6 30.0 %all_to_all.20 = bf16[16,128,384]{2,1,0:T(8,128)(2,1)S(1)} all-to-all(bf16[16,128,384]{2,1,0:T(8,128)(2,1)S(1)} %bitcast.29), channel_id=1, replica_groups=mesh['sp'=16,'dp'=8] {'sp'}, dimensions={0} | all-to-all | bytes 3145728 | tf_op jit(solution)/shard_map/all_to_all | solution.py:378
  31.7 0.0 copy-done.5
  31.7 0.0 copy-done.4
  31.7 0.0 copy-start
  31.7 0.0 copy-start.1
  31.7 0.0 copy-start.2
  31.7 7.6 %attention.1 = (bf16[2048,128]{1,0:T(8,128)(2,1)S(1)}, bf16[2048,2048]{1,0:T(8,128)(2,1)S(1)}, bf16[2048,1024]{1,0:T(8,128)(2,1)S(1)}, bf16[2048,1024]{1,0:T(8,128)(2,1)S(1)}, bf16[1024,2048]{1,0:T(8,128)(2,1)S(1)}) custom-call(f32[16]{0:T(128)S(1)} %copy-done.4, f32[1,128]{1,0:T(1,128)S(1)} %bitcast.39, bf16[2048,384]{1,0:T(8,128)(2,1)S(1)} %bitcast.28, ...), custom_call_target="tpu_custom_call" | custom-call | tf_op jit(solution)/shard_map/attention/pallas_call | solution.py:148
  39.3 13.3 %all_to_all.21 = bf16[16,128,128]{2,1,0:T(8,128)(2,1)S(1)} all-to-all(bf16[16,128,128]{2,1,0:T(8,128)(2,1)S(1)} %bitcast.34), channel_id=1, replica_groups=mesh['sp'=16,'dp'=8] {'sp'}, dimensions={0} | all-to-all | bytes 1048576 | tf_op jit(solution)/shard_map/all_to_all | solution.py:378
  52.6 0.0 copy-done
  52.6 0.0 copy-done.1
  52.6 0.0 copy-done.2
  52.6 2.4 %middle.1 = (f32[128,2048]{1,0:T(8,128)S(1)}, bf16[1024,1536]{1,0:T(8,128)(2,1)S(1)}) custom-call(bf16[2048,128]{1,0:T(8,128)(2,1)S(1)} %bitcast.32, bf16[2048,2048]{1,0:T(8,128)(2,1)S(1)} %get-tuple-element.15.weight_ref, bf16[128,2048]{1,0:T(8,128)(2,1)S(1)} %bitcast.33, f32[1,2048]{1,0:T(1,128)S(1)} %bitcast.37, s32[4,128]{1,0:T(4,128)S(1)} %bitcast.35), custom_call_target="tpu_custom_call" | custom-call | tf_op jit(solution)/shard_map/middle/pallas_call | solution.py:238
  55.0 0.0 copy-start.3
  55.0 48.8 %all_to_all.22 = bf16[128,8,1536]{2,1,0:T(8,128)(2,1)S(1)} all-to-all(bf16[128,8,1536]{2,1,0:T(8,128)(2,1)S(1)} %bitcast.31), channel_id=1, replica_groups=mesh['sp'=16,'dp'=8] {'sp','dp'}, dimensions={0} | all-to-all | bytes 6291456 | tf_op jit(solution)/shard_map/all_to_all | solution.py:378
  103.9 0.0 copy-done.3
  103.9 11.3 %experts.1 = (bf16[1024,1536]{1,0:T(8,128)(2,1)S(1)}, bf16[512,1024]{1,0:T(8,128)(2,1)S(1)}) custom-call(bf16[1024,1536]{1,0:T(8,128)(2,1)S(1)} %bitcast.26, bf16[2048,1024]{1,0:T(8,128)(2,1)S(1)} %get-tuple-element.18.gate_ref, bf16[2048,1024]{1,0:T(8,128)(2,1)S(1)} %get-tuple-element.19.up_ref, bf16[1024,2048]{1,0:T(8,128)(2,1)S(1)} %get-tuple-element.20.down_ref, ...), custom_call_target="tpu_custom_call" | custom-call | tf_op jit(solution)/shard_map/experts/pallas_call | solution.py:333
  115.2 45.6 %all_to_all.23 = bf16[128,8,1536]{2,1,0:T(8,128)(2,1)S(1)} all-to-all(bf16[128,8,1536]{2,1,0:T(8,128)(2,1)S(1)} %bitcast.30), channel_id=1, replica_groups=mesh['sp'=16,'dp'=8] {'sp','dp'}, dimensions={0} | all-to-all | bytes 6291456 | tf_op jit(solution)/shard_map/all_to_all | solution.py:378
  160.8 1.8 %combine.1 = bf16[128,2048]{1,0:T(8,128)(2,1)} custom-call(f32[128,2048]{1,0:T(8,128)S(1)} %get-tuple-element.16.mixed_ref, bf16[1024,1536]{1,0:T(8,128)(2,1)S(1)} %bitcast.27, bf16[512,1024]{1,0:T(8,128)(2,1)S(1)} %get-tuple-element.22.mix_ref), custom_call_target="tpu_custom_call" | custom-call | tf_op jit(solution)/shard_map/combine/pallas_call | solution.py:366
Async XLA Ops:
  0.0 31.7 %copy-start.5 = (f32[128]{0:T(128)S(1)}, f32[128]{0:T(128)}, u32[]{:S(2)}) copy-start(f32[128]{0:T(128)} %param.21) | copy-start | bytes 1540
  0.0 31.7 %copy-start.4 = (f32[16]{0:T(128)S(1)}, f32[16]{0:T(128)}, u32[]{:S(2)}) copy-start(f32[16]{0:T(128)} %lam_ref.1) | copy-start | bytes 196
  31.7 20.9 %copy-start = (bf16[1,128,2048]{2,1,0:T(8,128)(2,1)S(1)}, bf16[1,128,2048]{2,1,0:T(8,128)(2,1)}, u32[]{:S(2)}) copy-start(bf16[1,128,2048]{2,1,0:T(8,128)(2,1)} %param.22) | copy-start | bytes 1572868
  31.7 20.9 %copy-start.1 = (s32[1,128,4]{1,2,0:T(4,128)S(1)}, s32[1,128,4]{1,2,0:T(4,128)}, u32[]{:S(2)}) copy-start(s32[1,128,4]{1,2,0:T(4,128)} %param.25) | copy-start | bytes 6148
  31.7 20.9 %copy-start.2 = (f32[2048]{0:T(1024)S(1)}, f32[2048]{0:T(1024)}, u32[]{:S(2)}) copy-start(f32[2048]{0:T(1024)} %param.24) | copy-start | bytes 24580
  55.0 48.8 %copy-start.3 = (f32[1,128,4]{1,2,0:T(4,128)S(1)}, f32[1,128,4]{1,2,0:T(4,128)}, u32[]{:S(2)}) copy-start(f32[1,128,4]{1,2,0:T(4,128)} %param.26) | copy-start | bytes 6148
